TPU v7x, 32 devices: a whole 2x2x4 slice. The times are simulated.
32 devices in a mesh: sp: 8 (over z, y), tp: 4 (over x, core).
Axes of the slice: x: 2, y: 2, z: 4, core: 2. Of those that a mesh axis runs over, the one named last changes fastest.
Arguments:
- tokens: bfloat16 [4096, 2048], P('sp'), may hold values from -6 to 6
- input_norm_gain: bfloat16 [2048], replicated, may hold values from 0.099609375 to 1.8984375
- gate_matrix: bfloat16 [2048, 1024], P('sp', 'tp'), may hold values from -0.125 to 0.125
- input_matrix: bfloat16 [2048, 1024], P('sp', 'tp'), may hold values from -0.125 to 0.125
- write_matrix: bfloat16 [2048, 512], P('sp', 'tp'), may hold values from -0.125 to 0.125
- read_matrix: bfloat16 [2048, 512], P('sp', 'tp'), may hold values from -0.125 to 0.125
- step_matrix: bfloat16 [2048, 16], P('sp'), may hold values from -0.125 to 0.125
- pooling_input_matrix: bfloat16 [2048, 1024], P('sp', 'tp'), may hold values from -0.125 to 0.125
- input_conv_taps: bfloat16 [3, 1024], P(None, 'tp'), may hold values from -3.5 to 3.5
- write_conv_taps: bfloat16 [3, 512], P(None, 'tp'), may hold values from -3.5 to 3.5
- read_conv_taps: bfloat16 [3, 512], P(None, 'tp'), may hold values from -3.5 to 3.5
- head_step_base: float32 [16], P('tp'), may hold values from 0 to 1, as said below
- position_step_factor: float32 [4096], P('sp'), may hold values from 0 to 3, as said below
- position_log_decay: float32 [4096, 16], P('sp', 'tp'), may hold values from -2 to 0, as said below
- gated_norm_gain: bfloat16 [1024], P('tp'), may hold values from 0.099609375 to 1.8984375
- group_linear_maps: bfloat16 [4, 256, 256], P('tp'), may hold values from -0.375 to 0.375
- pooling_channel_scale: bfloat16 [1024], P('tp'), may hold values from 0.099609375 to 1.8984375
- state_output_matrix: bfloat16 [1024, 2048], P('tp', 'sp'), may hold values from -0.125 to 0.125
- pooling_output_matrix: bfloat16 [1024, 2048], P('tp', 'sp'), may hold values from -0.125 to 0.125
Outputs:
- mixed: bfloat16 [4096, 2048], P(('sp', 'tp'))
Inputs may be any that keep to these rules, and one draw needn't show every extreme that they name: `head_step_base`: positive. `position_step_factor`: positive. `position_log_decay`: never positive.
All inputs are finite; a program needn't handle non-finite values.
Results may differ from a plain program's by a relative error of at most 0.012.
Values may be sent and summed in bfloat16 or wider, within the bound.
A program may use at most 64 MiB of HBM per device.

v0:
```python
import jax
import jax.numpy as jnp
from jax import lax
from jax.sharding import PartitionSpec as P

SSD_INNER = 1024
HEAD_DIM = 64
STATE = 128
POOL_WIDTH = 1024
POOL_GROUPS = 4
BLOCK = 128


EPSILON = 1e-06


def extended_2(array, sides, width):
    for axis, dim in sides:
        size, length = (lax.axis_size(axis), array.shape[dim])
        up = [(i, (i + 1) % size) for i in range(size - 1)]
        down = [(j, i) for i, j in up]
        last = lax.slice_in_dim(array, length - width, length, axis=dim)
        initial = lax.slice_in_dim(array, 0, width, axis=dim)
        before = lax.ppermute(last, axis, up)
        after = lax.ppermute(initial, axis, down)
        array = jnp.concatenate([before, array, after], axis=dim)
    return array


def entering_2(array, axis, combine, identity, reverse):
    size, position = (lax.axis_size(axis), lax.axis_index(axis))
    everything = jax.tree.map(lambda part: lax.all_gather(part, axis), array)
    start = jax.tree.map(
        lambda part, zero: jnp.broadcast_to(jnp.asarray(zero, part.dtype), part.shape),
        array,
        identity,
    )

    def step(k, before):
        at = size - 1 - k if reverse else k
        reached = at > position if reverse else at < position
        new = combine(before, jax.tree.map(lambda part: part[at], everything))
        return jax.tree.map(lambda a, b: jnp.where(reached, a, b), new, before)

    return lax.fori_loop(0, size, step, start)


def block_sweep(readers, writers, values, decay_logarithm):
    f32 = jnp.float32
    length = values.shape[0]
    blocks = length // BLOCK
    lower_mask = jnp.tril(jnp.ones((BLOCK, BLOCK), dtype=bool))[:, :, None, None]

    def as_blocks(array):
        return array.reshape((blocks, BLOCK) + array.shape[1:])

    def one_block(carry_state, inputs):
        read_block, write_block, value_block, decay_block = inputs
        running = jnp.cumsum(decay_block, axis=0)
        scores = jnp.einsum("ign,jgn->ijg", read_block, write_block, preferred_element_type=f32)
        spread = jnp.where(lower_mask, running[:, None] - running[None, :], -jnp.inf)
        weights = scores[..., None] * jnp.exp(spread)
        within = jnp.einsum("ijgr,jgrp->igrp", weights, value_block, preferred_element_type=f32)
        carried = jnp.einsum("ign,grnp->igrp", read_block, carry_state, preferred_element_type=f32)
        carried = carried * jnp.exp(running)[..., None]
        block_total = running[-1]
        fading = jnp.exp(block_total[None] - running)
        inflow = jnp.einsum(
            "jgn,jgrp->grnp",
            write_block,
            value_block * fading[..., None],
            preferred_element_type=f32,
        )
        return (carry_state * jnp.exp(block_total)[..., None, None] + inflow, within + carried)

    initial = jnp.zeros((values.shape[1], values.shape[2], writers.shape[2], values.shape[3]), f32)
    last_state, outputs = lax.scan(
        one_block,
        initial,
        (as_blocks(readers), as_blocks(writers), as_blocks(values), as_blocks(decay_logarithm)),
    )
    return (outputs.reshape(values.shape), last_state)


def link(earlier, later):
    return (earlier[0] + later[0], earlier[1] * jnp.exp(later[0])[..., None, None] + later[1])


def shards(
    tokens,
    input_norm_gain,
    gate_matrix,
    input_matrix,
    write_matrix,
    read_matrix,
    step_matrix,
    pooling_input_matrix,
    input_conv_taps,
    write_conv_taps,
    read_conv_taps,
    head_step_base,
    position_step_factor,
    position_log_decay,
    gated_norm_gain,
    group_linear_maps,
    pooling_channel_scale,
    state_output_matrix,
    pooling_output_matrix,
):
    f32 = jnp.float32
    bf16 = jnp.bfloat16
    local_rows = tokens.shape[0]
    seq_devices = lax.axis_size("sp")
    seq_index = lax.axis_index("sp")
    head_index = lax.axis_index("tp")
    wide = tokens.astype(f32)
    normed = (
        wide
        * lax.rsqrt(jnp.mean(wide * wide, axis=1, keepdims=True) + EPSILON)
        * input_norm_gain.astype(f32)
    ).astype(bf16)
    pieces = (
        lax.all_gather(gate_matrix, "sp", axis=0, tiled=True),
        lax.all_gather(input_matrix, "sp", axis=0, tiled=True),
        lax.all_gather(write_matrix, "sp", axis=0, tiled=True),
        lax.all_gather(read_matrix, "sp", axis=0, tiled=True),
        lax.all_gather(step_matrix, "sp", axis=0, tiled=True),
        lax.all_gather(pooling_input_matrix, "sp", axis=0, tiled=True),
    )
    gate_pre, input_pre, write_pre, read_pre, step_raw, pool_acc = tuple(
        (jnp.dot(normed, piece, preferred_element_type=f32) for piece in pieces)
    )
    inner_here = input_pre.shape[1]
    state_here = write_pre.shape[1]
    conv_in = jnp.concatenate((input_pre, write_pre, read_pre), axis=1).astype(bf16)
    padded = extended_2(conv_in, (("sp", 0),), 1)
    taps = jnp.concatenate((input_conv_taps, write_conv_taps, read_conv_taps), axis=1).astype(f32)
    conv_out = (
        padded[0:local_rows] * taps[0]
        + padded[1 : local_rows + 1] * taps[1]
        + padded[2 : local_rows + 2] * taps[2]
    )
    activated = jax.nn.silu(conv_out).astype(bf16)
    inputs = activated[:, :inner_here]
    writers = activated[:, inner_here : inner_here + state_here]
    readers = activated[:, inner_here + state_here :]
    heads_here = inner_here // HEAD_DIM
    local_groups = state_here // STATE
    repeat_count = heads_here // local_groups
    step_own = lax.dynamic_slice_in_dim(step_raw, head_index * heads_here, heads_here, 1)
    step_size = head_step_base[None, :] * jax.nn.softplus(step_own) * position_step_factor[:, None]
    decay_logarithm = (position_log_decay - step_size).reshape(
        local_rows, local_groups, repeat_count
    )
    values = (
        inputs.astype(f32).reshape(local_rows, heads_here, HEAD_DIM) * step_size[..., None]
    ).reshape(local_rows, local_groups, repeat_count, HEAD_DIM)
    readers_g = readers.reshape(local_rows, local_groups, STATE)
    writers_g = writers.reshape(local_rows, local_groups, STATE)
    readers_back = jnp.flip(readers_g, 0)
    decay_back = jnp.flip(decay_logarithm, 0)
    local_ahead, state_ahead = block_sweep(readers_g, writers_g, values, decay_logarithm)
    local_behind, state_behind = block_sweep(
        readers_back, jnp.flip(writers_g, 0), jnp.flip(values, 0), decay_back
    )
    totals = jnp.sum(decay_logarithm, axis=0)
    identity = (jnp.zeros_like(totals), jnp.zeros_like(state_ahead))
    entering = entering_2((totals, state_ahead), "sp", link, identity, False)[1]
    leaving = entering_2((totals, state_behind), "sp", link, identity, True)[1]
    extra_ahead = (
        jnp.einsum("tgn,grnp->tgrp", readers_g, entering, preferred_element_type=f32)
        * jnp.exp(jnp.cumsum(decay_logarithm, axis=0))[..., None]
    )
    extra_behind = (
        jnp.einsum("tgn,grnp->tgrp", readers_back, leaving, preferred_element_type=f32)
        * jnp.exp(jnp.cumsum(decay_back, axis=0))[..., None]
    )
    scanned = (local_ahead + extra_ahead + jnp.flip(local_behind + extra_behind, 0)).reshape(
        local_rows, inner_here
    )
    gated = scanned * jax.nn.silu(gate_pre.astype(bf16).astype(f32))
    squares = lax.psum(jnp.sum(gated * gated, axis=1), "tp")
    state_mixed = (
        gated * lax.rsqrt(squares / SSD_INNER + EPSILON)[:, None] * gated_norm_gain.astype(f32)
    ).astype(bf16)
    pool_in = pool_acc.astype(bf16)
    reach = 2 ** (POOL_GROUPS - 1)
    width_group = POOL_WIDTH // POOL_GROUPS
    groups_pool = pool_in.shape[1] // width_group
    extended = extended_2(pool_in, (("sp", 0),), reach)
    group_ids = head_index * groups_pool + lax.iota(jnp.int32, groups_pool)
    halves = jnp.left_shift(jnp.ones_like(group_ids), group_ids)
    window_sum = jnp.zeros((local_rows, groups_pool, width_group), f32)
    for offset in range(-reach, reach):
        taken = ((offset >= -halves) & (offset < halves)).astype(f32)
        shifted = (
            extended[reach + offset : reach + offset + local_rows]
            .astype(f32)
            .reshape(local_rows, groups_pool, width_group)
        )
        window_sum = window_sum + shifted * taken[None, :, None]
    positions = (seq_index * local_rows + lax.iota(jnp.int32, local_rows))[:, None]
    counts = (
        jnp.minimum(positions + halves[None, :], local_rows * seq_devices)
        - jnp.maximum(positions - halves[None, :], 0)
    ).astype(f32)
    pooled = (
        window_sum / counts[..., None]
        - pool_in.astype(f32).reshape(local_rows, groups_pool, width_group)
    ).astype(bf16)
    mapped = jnp.einsum("tgc,gcd->tgd", pooled, group_linear_maps, preferred_element_type=f32)
    pool_mixed = (
        mapped.reshape(local_rows, groups_pool * width_group) * pooling_channel_scale.astype(f32)
    ).astype(bf16)
    state_cols, pool_cols = (
        lax.all_gather(state_output_matrix, "sp", axis=1, tiled=True),
        lax.all_gather(pooling_output_matrix, "sp", axis=1, tiled=True),
    )
    state_rows, pool_rows = (
        lax.all_to_all(state_mixed, "tp", split_axis=0, concat_axis=1, tiled=True),
        lax.all_to_all(pool_mixed, "tp", split_axis=0, concat_axis=1, tiled=True),
    )
    state_full, pool_full = (
        lax.all_gather(state_cols, "tp", axis=0, tiled=True),
        lax.all_gather(pool_cols, "tp", axis=0, tiled=True),
    )
    summed = jnp.dot(state_rows, state_full, preferred_element_type=f32) + jnp.dot(
        pool_rows, pool_full, preferred_element_type=f32
    )
    return summed.astype(bf16)


def solution(mesh):
    placed = (
        P("sp", None),
        P(),
        P("sp", "tp"),
        P("sp", "tp"),
        P("sp", "tp"),
        P("sp", "tp"),
        P("sp", None),
        P("sp", "tp"),
        P(None, "tp"),
        P(None, "tp"),
        P(None, "tp"),
        P("tp"),
        P("sp"),
        P("sp", "tp"),
        P("tp"),
        P("tp", None, None),
        P("tp"),
        P("tp", "sp"),
        P("tp", "sp"),
    )
    return jax.shard_map(
        shards, mesh=mesh, in_specs=placed, out_specs=P(("sp", "tp"), None), check_vma=False
    )
```

profile of v0, /device:TPU:1, one launch (start us, length us, event | category | flops | bytes accessed | tf_op | source)
XLA Modules:
  0.0 391.7 jit_solution(2515644345945067604)
XLA Ops:
  12.3 27.2 %all_gather.53 = bf16[2048,128]{1,0:T(8,128)(2,1)S(1)} all-gather(bf16[256,128]{1,0:T(8,128)(2,1)S(1)} %copy-done.14), channel_id=1, replica_groups=mesh['sp'=8,'tp'=4] {'sp'}, dimensions={0}, use_global_device_ids=true | all-gather | bytes 589824 | tf_op jit(solution)/shard_map/all_gather | solution.py:126
  39.6 26.4 %all_gather.52 = bf16[2048,128]{1,0:T(8,128)(2,1)S(1)} all-gather(bf16[256,128]{1,0:T(8,128)(2,1)S(1)} %copy-done.15), channel_id=1, replica_groups=mesh['sp'=8,'tp'=4] {'sp'}, dimensions={0}, use_global_device_ids=true | all-gather | bytes 589824 | tf_op jit(solution)/shard_map/all_gather | solution.py:125
  68.2 24.3 %all_gather.50 = bf16[2048,16]{0,1:T(8,128)(2,1)S(1)} all-gather(bf16[256,16]{0,1:T(8,128)(2,1)S(1)} %copy-done.16), channel_id=1, replica_groups=mesh['sp'=8,'tp'=4] {'sp'}, dimensions={0}, use_global_device_ids=true | all-gather | bytes 73728 | tf_op jit(solution)/shard_map/all_gather | solution.py:127
  120.3 39.7 %while.58 = (s32[]{:T(128)}, f32[1,4,128,64]{2,3,1,0:T(8,128)S(1)}, f32[4,128,1,4,64]{1,0,4,3,2:T(4,128)}, f32[4,128,1,4]{3,1,2,0:T(8,128)}, f32[4,128,1,4,64]{1...) while((s32[]{:T(128)}, f32[1,4,128,64]{2,3,1,0:T(8,128)S(1)}, ...), condition=%wide.region_11.12_spmd.clone, body=%wide.region_9.11_spmd.clone.sunk | while | flops 29835268 | bytes 2287827 | solution.py:77
  124.9 4.4 %dynamic_update_slice.12 = f32[4,128,1,4,64]{1,0,4,3,2:T(4,128)} dynamic-update-slice(f32[4,128,1,4,64]{1,0,4,3,2:T(4,128)} %get-tuple-element.740, f32[1,128,1,4,64]{1,0,4,3,2:T(1,128)S(1)} %bitcast.368, s32[]{:T(128)} %get-tuple-element.738, s32[]{:T(128)} %constant.182.clone.1..sunk.2, s32[]{:T(128)} %constant.182.clone.1..sunk.2, s32[]{:T(128)} %constant.182.clone.1..sunk.2, ...) | dynamic-update-slice | bytes 262148 | tf_op jit(solution)/shard_map/while/body/jit(dynamic_update_index_in_dim)/dynamic_update_slice | solution.py:77
  134.8 4.4 %dynamic_update_slice.12 = f32[4,128,1,4,64]{1,0,4,3,2:T(4,128)} dynamic-update-slice(f32[4,128,1,4,64]{1,0,4,3,2:T(4,128)} %get-tuple-element.740, f32[1,128,1,4,64]{1,0,4,3,2:T(1,128)S(1)} %bitcast.368, s32[]{:T(128)} %get-tuple-element.738, s32[]{:T(128)} %constant.182.clone.1..sunk.2, s32[]{:T(128)} %constant.182.clone.1..sunk.2, s32[]{:T(128)} %constant.182.clone.1..sunk.2, ...) | dynamic-update-slice | bytes 262148 | tf_op jit(solution)/shard_map/while/body/jit(dynamic_update_index_in_dim)/dynamic_update_slice | solution.py:77
  144.8 4.4 %dynamic_update_slice.12 = f32[4,128,1,4,64]{1,0,4,3,2:T(4,128)} dynamic-update-slice(f32[4,128,1,4,64]{1,0,4,3,2:T(4,128)} %get-tuple-element.740, f32[1,128,1,4,64]{1,0,4,3,2:T(1,128)S(1)} %bitcast.368, s32[]{:T(128)} %get-tuple-element.738, s32[]{:T(128)} %constant.182.clone.1..sunk.2, s32[]{:T(128)} %constant.182.clone.1..sunk.2, s32[]{:T(128)} %constant.182.clone.1..sunk.2, ...) | dynamic-update-slice | bytes 262148 | tf_op jit(solution)/shard_map/while/body/jit(dynamic_update_index_in_dim)/dynamic_update_slice | solution.py:77
  154.7 4.4 %dynamic_update_slice.12 = f32[4,128,1,4,64]{1,0,4,3,2:T(4,128)} dynamic-update-slice(f32[4,128,1,4,64]{1,0,4,3,2:T(4,128)} %get-tuple-element.740, f32[1,128,1,4,64]{1,0,4,3,2:T(1,128)S(1)} %bitcast.368, s32[]{:T(128)} %get-tuple-element.738, s32[]{:T(128)} %constant.182.clone.1..sunk.2, s32[]{:T(128)} %constant.182.clone.1..sunk.2, s32[]{:T(128)} %constant.182.clone.1..sunk.2, ...) | dynamic-update-slice | bytes 262148 | tf_op jit(solution)/shard_map/while/body/jit(dynamic_update_index_in_dim)/dynamic_update_slice | solution.py:77
  165.1 30.7 %while.56 = (s32[]{:T(128)}, f32[1,4,128,64]{2,3,1,0:T(8,128)S(1)}, f32[4,128,1,4,64]{1,0,4,3,2:T(4,128)}, f32[4,128,1,4]{3,1,2,0:T(8,128)}, f32[4,128,1,4,64]{1...) while((s32[]{:T(128)}, f32[1,4,128,64]{2,3,1,0:T(8,128)S(1)}, ...), condition=%wide.region_3.4_spmd.clone, body=%wide.region_1.3_spmd.clone.sunk | while | flops 29835268 | bytes 1962695 | solution.py:77
  168.2 4.4 %dynamic_update_slice.11 = f32[4,128,1,4,64]{1,0,4,3,2:T(4,128)} dynamic-update-slice(f32[4,128,1,4,64]{1,0,4,3,2:T(4,128)} %get-tuple-element.794, f32[1,128,1,4,64]{1,0,4,3,2:T(1,128)S(1)} %bitcast.372, s32[]{:T(128)} %get-tuple-element.792, s32[]{:T(128)} %constant.182.clone.1..sunk, s32[]{:T(128)} %constant.182.clone.1..sunk, s32[]{:T(128)} %constant.182.clone.1..sunk, s32[]{:T(128)} %constant.182.clone.1..sunk) | dynamic-update-slice | bytes 262148 | tf_op jit(solution)/shard_map/while/body/jit(dynamic_update_index_in_dim)/dynamic_update_slice | solution.py:77
  175.9 4.4 %dynamic_update_slice.11 = f32[4,128,1,4,64]{1,0,4,3,2:T(4,128)} dynamic-update-slice(f32[4,128,1,4,64]{1,0,4,3,2:T(4,128)} %get-tuple-element.794, f32[1,128,1,4,64]{1,0,4,3,2:T(1,128)S(1)} %bitcast.372, s32[]{:T(128)} %get-tuple-element.792, s32[]{:T(128)} %constant.182.clone.1..sunk, s32[]{:T(128)} %constant.182.clone.1..sunk, s32[]{:T(128)} %constant.182.clone.1..sunk, s32[]{:T(128)} %constant.182.clone.1..sunk) | dynamic-update-slice | bytes 262148 | tf_op jit(solution)/shard_map/while/body/jit(dynamic_update_index_in_dim)/dynamic_update_slice | solution.py:77
  183.6 4.4 %dynamic_update_slice.11 = f32[4,128,1,4,64]{1,0,4,3,2:T(4,128)} dynamic-update-slice(f32[4,128,1,4,64]{1,0,4,3,2:T(4,128)} %get-tuple-element.794, f32[1,128,1,4,64]{1,0,4,3,2:T(1,128)S(1)} %bitcast.372, s32[]{:T(128)} %get-tuple-element.792, s32[]{:T(128)} %constant.182.clone.1..sunk, s32[]{:T(128)} %constant.182.clone.1..sunk, s32[]{:T(128)} %constant.182.clone.1..sunk, s32[]{:T(128)} %constant.182.clone.1..sunk) | dynamic-update-slice | bytes 262148 | tf_op jit(solution)/shard_map/while/body/jit(dynamic_update_index_in_dim)/dynamic_update_slice | solution.py:77
  191.2 4.4 %dynamic_update_slice.11 = f32[4,128,1,4,64]{1,0,4,3,2:T(4,128)} dynamic-update-slice(f32[4,128,1,4,64]{1,0,4,3,2:T(4,128)} %get-tuple-element.794, f32[1,128,1,4,64]{1,0,4,3,2:T(1,128)S(1)} %bitcast.372, s32[]{:T(128)} %get-tuple-element.792, s32[]{:T(128)} %constant.182.clone.1..sunk, s32[]{:T(128)} %constant.182.clone.1..sunk, s32[]{:T(128)} %constant.182.clone.1..sunk, s32[]{:T(128)} %constant.182.clone.1..sunk) | dynamic-update-slice | bytes 262148 | tf_op jit(solution)/shard_map/while/body/jit(dynamic_update_index_in_dim)/dynamic_update_slice | solution.py:77
  209.9 17.8 %all-reduce = f32[32]{0:T(128)S(1)} all-reduce(f32[32]{0:T(128)S(1)} %dynamic-update-slice), channel_id=2, replica_groups=mesh['sp'=8,'tp'=4] {'sp'}, use_global_device_ids=true, to_apply=%add | all-reduce | flops 32 | bytes 256
  231.1 6.1 %fusion.103 = f32[512,256]{1,0:T(8,128)S(1)} fusion(bf16[512,256]{1,0:T(8,128)(2,1)} %copy-done.24, bf16[8,256]{1,0:T(8,128)(2,1)S(1)} %collective-permute-done.3, bf16[8,256]{1,0:T(8,128)(2,1)S(1)} %collective-permute-done.2, f32[512]{0:T(512)S(1)} %subtract_convert_fusion, f32[]{:T(128)S(6)} %mul.542, f32[]{:T(128)S(6)} %mul.539, f32[]{:T(128)S(6)} %mul.536, ...), kind=kOutput, calls=%fused_computation.177 | convolution fusion | flops 79560704 | bytes 927808 | tf_op jit(solution)/shard_map/tgc,gcd->tgd/dot_general | solution.py:211
  238.2 9.7 %while.59 = (s32[]{:T(128)}, f32[1,4,128,64]{3,2,1,0:T(8,128)S(1)}, s32[]{:T(128)}, f32[8,1,4]{2,1,0:T(1,128)S(1)}, f32[8,1,4,128,64]{3,4,2,0,1:T(8,128)}, /*index=5*/s32[]{:T(128)}, s32[]{:T(128)}, s32[]{:T(128)}, s32[]{:T(128)}) while((s32[]{:T(128)}, f32[1,4,128,64]{3,2,1,0:T(8,128)S(1)}, s32[]{:T(128)}, ...), condition=%wide.region_13.14_spmd.clone, body=%wide.region_12.13_spmd.clone.sunk | while | flops 131080 | bytes 917719 | solution.py:45
  250.9 10.8 %all-gather.27.cloned.1.call-done = f32[8,4,128,64]{2,3,1,0:T(8,128)} async-done(((f32[1,4,128,64]{2,3,1,0:T(8,128)}), f32[8,4,128,64]{2,3,1,0:T(8,128)}) %all-gather.27.cloned.1.call-update) | async-done | bytes 1048592 | tf_op jit(solution)/shard_map/all_gather | solution.py:32
  261.7 9.7 %while.57 = (s32[]{:T(128)}, f32[1,4,128,64]{3,2,1,0:T(8,128)S(1)}, s32[]{:T(128)}, f32[8,1,4]{2,1,0:T(1,128)S(1)}, f32[8,1,4,128,64]{3,4,2,0,1:T(8,128)}, /*index=5*/s32[]{:T(128)}, s32[]{:T(128)}) while((s32[]{:T(128)}, f32[1,4,128,64]{3,2,1,0:T(8,128)S(1)}, s32[]{:T(128)}, f32[8,1,4]{2,1,0:T(1,128)S(1)}, ...), condition=%wide.region_6.7_spmd.clone, body=%wide.region_5.6_spmd.clone.sunk | while | flops 131076 | bytes 917657 | solution.py:45
  274.8 28.1 %all-gather.15.cloned.1.call-done = bf16[2048,256]{1,0:T(8,128)(2,1)} async-done(((bf16[256,256]{1,0:T(8,128)(2,1)}), bf16[2048,256]{1,0:T(8,128)(2,1)}) %all-gather.15.cloned.1.call-update) | async-done | bytes 1048592 | tf_op jit(solution)/shard_map/all_gather | solution.py:123
  304.9 7.5 %psum.7 = f32[512]{0:T(512)S(1)} all-reduce(f32[512]{0:T(512)S(1)} %get-tuple-element.571), channel_id=1, replica_groups=mesh['sp'=8,'tp'=4] {'tp'}, use_global_device_ids=true, to_apply=%region_17.18 | all-reduce | flops 512 | bytes 4096 | tf_op jit(solution)/shard_map/psum | solution.py:182
  318.3 7.7 %all-to-all-done = bf16[4,128,256]{1,2,0:T(8,128)(2,1)S(1)} async-done(((bf16[4,128,256]{1,2,0:T(8,128)(2,1)}), bf16[4,128,256]{1,2,0:T(8,128)(2,1)S(1)}, u32[]{:S(2)}, u32[]{:S(2)}) %all-to-all-start) | async-done | bytes 262176 | tf_op jit(solution)/shard_map/all_to_all | solution.py:220
  326.0 4.1 %all-to-all-start.1 = ((bf16[4,128,256]{1,2,0:T(8,128)(2,1)}), bf16[4,128,256]{1,2,0:T(8,128)(2,1)S(1)}, u32[]{:S(2)}, u32[]{:S(2)}) async-start(bf16[4,128,256]{1,2,0:T(8,128)(2,1)} %multiply_convert_fusion.1), calls=%async_computation.1 | async-start | bytes 524288 | tf_op jit(solution)/shard_map/all_to_all | solution.py:221
  330.1 15.3 %all-gather.19.cloned.1.call-done = bf16[1024,2048]{1,0:T(8,128)(2,1)} async-done(((bf16[256,2048]{1,0:T(8,128)(2,1)}), bf16[1024,2048]{1,0:T(8,128)(2,1)}) %all-gather.19.cloned.1.call-update) | async-done | bytes 4194320 | tf_op jit(solution)/shard_map/all_gather | solution.py:224
  348.3 33.1 %all-gather.25.cloned.1.call-done = bf16[1024,2048]{1,0:T(8,128)(2,1)} async-done(((bf16[256,2048]{1,0:T(8,128)(2,1)}), bf16[1024,2048]{1,0:T(8,128)(2,1)}) %all-gather.25.cloned.1.call-update) | async-done | bytes 4194320 | tf_op jit(solution)/shard_map/all_gather | solution.py:225
  (337 shorter events, 132.6 us)
Async XLA Ops:
  6.5 224.5 %copy-start = (bf16[1,256,256]{2,1,0:T(8,128)(2,1)S(1)}, bf16[1,256,256]{2,1,0:T(8,128)(2,1)}, u32[]{:S(2)}) copy-start(bf16[1,256,256]{2,1,0:T(8,128)(2,1)} %param.42) | copy-start | bytes 393220
  6.5 33.0 %copy-start.15 = (bf16[256,128]{1,0:T(8,128)(2,1)S(1)}, bf16[256,128]{1,0:T(8,128)(2,1)}, u32[]{:S(2)}) copy-start(bf16[256,128]{1,0:T(8,128)(2,1)} %param.31) | copy-start | bytes 196612
  6.5 87.4 %all-gather.13.cloned.1.call-start = ((), (), s32[]{:S(2)}) async-start(), calls=%async_computation.2 | async-start | bytes 1179648 | tf_op jit(solution)/shard_map/all_gather | solution.py:124
  7.3 190.0 %all-gather.17.cloned.1.call-start = ((), (), s32[]{:S(2)}) async-start(), calls=%async_computation.4 | async-start | bytes 1179648 | tf_op jit(solution)/shard_map/all_gather | solution.py:216
  8.0 194.2 %all-gather.21.cloned.1.call-start = ((), (), s32[]{:S(2)}) async-start(), calls=%async_computation.6 | async-start | bytes 1179648 | tf_op jit(solution)/shard_map/all_gather | solution.py:128
  8.7 219.2 %all-gather.23.cloned.1.call-start = ((), (), s32[]{:S(2)}) async-start(), calls=%async_computation.7 | async-start | bytes 1179648 | tf_op jit(solution)/shard_map/all_gather | solution.py:217
  9.3 228.8 %all-gather.29.cloned.1.call-start = ((), (), s32[]{:S(2)}) async-start(), calls=%async_computation.10 | async-start | bytes 1179648 | tf_op jit(solution)/shard_map/all_gather | solution.py:32
  9.4 56.6 %copy-start.1 = (bf16[512,2048]{1,0:T(8,128)(2,1)S(1)}, bf16[512,2048]{1,0:T(8,128)(2,1)}, u32[]{:S(2)}) copy-start(bf16[512,2048]{1,0:T(8,128)(2,1)} %param.27) | copy-start | bytes 6291460
  67.3 25.9 %copy-start.17 = (f32[512,4]{0,1:T(4,128)S(1)}, f32[512,4]{0,1:T(4,128)}, u32[]{:S(2)}) copy-start(f32[512,4]{0,1:T(4,128)} %param.40) | copy-start | bytes 24580
  67.3 25.9 %copy-start.18 = (f32[512]{0:T(512)S(1)}, f32[512]{0:T(512)}, u32[]{:S(2)}) copy-start(f32[512]{0:T(512)} %param.39) | copy-start | bytes 6148
  67.4 25.9 %copy-start.22 = (f32[4]{0:T(128)S(1)}, f32[4]{0:T(128)}, u32[]{:S(2)}) copy-start(f32[4]{0:T(128)} %param.38) | copy-start | bytes 52
  96.1 7.5 %collective-permute-start = (bf16[1,512]{0,1:T(8,128)(2,1)S(1)}, bf16[1,512]{0,1:T(8,128)(2,1)S(1)}, u32[]{:S(2)}, u32[]{:S(2)}) collective-permute-start(bf16[1,512]{0,1:T(8,128)(2,1)S(1)} %get-tuple-element.564), channel_id=1, source_target_pairs={{0,4},{4,8},{8,12},{12,16},{16,20},{20,24},{24,28},{1,5},{5,9},{9,... | collective-permute-start | bytes 3080 | tf_op jit(solution)/shard_map/ppermute | solution.py:24
  99.6 5.8 %collective-permute-start.1 = (bf16[1,512]{0,1:T(8,128)(2,1)S(1)}, bf16[1,512]{0,1:T(8,128)(2,1)S(1)}, u32[]{:S(2)}, u32[]{:S(2)}) collective-permute-start(bf16[1,512]{0,1:T(8,128)(2,1)S(1)} %get-tuple-element.565), channel_id=1, source_target_pairs={{4,0},{8,4},{12,8},{16,12},{20,16},{24,20},{28,24},{5,1},{9,5},{13... | collective-permute-start | bytes 3080 | tf_op jit(solution)/shard_map/ppermute | solution.py:25
  163.1 98.6 %all-gather.27.cloned.1.call-start = ((), (), s32[]{:S(2)}) async-start(), calls=%async_computation.9 | async-start | bytes 1179648 | tf_op jit(solution)/shard_map/all_gather | solution.py:32
  165.1 35.3 %copy-start.11 = (f32[512,4]{0,1:T(4,128)S(1)}, f32[512,4]{0,1:T(4,128)}, u32[]{:S(2)}) copy-start(f32[512,4]{0,1:T(4,128)} %copy-done.10) | copy-start | bytes 24580
  196.5 106.4 %all-gather.15.cloned.1.call-start = ((), (), s32[]{:S(2)}) async-start(), calls=%async_computation.3 | async-start | bytes 1179648 | tf_op jit(solution)/shard_map/all_gather | solution.py:123
  197.2 148.1 %all-gather.19.cloned.1.call-start = ((), (), s32[]{:S(2)}) async-start(), calls=%async_computation.5 | async-start | bytes 5242880 | tf_op jit(solution)/shard_map/all_gather | solution.py:224
  198.0 183.4 %all-gather.25.cloned.1.call-start = ((), (), s32[]{:S(2)}) async-start(), calls=%async_computation.8 | async-start | bytes 5242880 | tf_op jit(solution)/shard_map/all_gather | solution.py:225
  200.0 27.8 %copy-start.25 = (bf16[256]{0:T(256)(128)(2,1)S(1)}, bf16[256]{0:T(256)(128)(2,1)}, u32[]{:S(2)}) copy-start(bf16[256]{0:T(256)(128)(2,1)} %param.41) | copy-start | bytes 1540
  200.5 27.4 %copy-start.26 = (bf16[256]{0:T(256)(128)(2,1)S(1)}, bf16[256]{0:T(256)(128)(2,1)}, u32[]{:S(2)}) copy-start(bf16[256]{0:T(256)(128)(2,1)} %param.43) | copy-start | bytes 1540
  204.3 26.8 %collective-permute-start.2 = (bf16[8,256]{1,0:T(8,128)(2,1)S(1)}, bf16[8,256]{1,0:T(8,128)(2,1)S(1)}, u32[]{:S(2)}, u32[]{:S(2)}) collective-permute-start(bf16[8,256]{1,0:T(8,128)(2,1)S(1)} %get-tuple-element.566), channel_id=1, source_target_pairs={{0,4},{4,8},{8,12},{12,16},{16,20},{20,24},{24,28},{1,5},{5,9},{9,... | collective-permute-start | bytes 12296 | tf_op jit(solution)/shard_map/ppermute | solution.py:24
  207.0 24.0 %collective-permute-start.3 = (bf16[8,256]{1,0:T(8,128)(2,1)S(1)}, bf16[8,256]{1,0:T(8,128)(2,1)S(1)}, u32[]{:S(2)}, u32[]{:S(2)}) collective-permute-start(bf16[8,256]{1,0:T(8,128)(2,1)S(1)} %get-tuple-element.567), channel_id=1, source_target_pairs={{4,0},{8,4},{12,8},{16,12},{20,16},{24,20},{28,24},{5,1},{9,5},{13... | collective-permute-start | bytes 12296 | tf_op jit(solution)/shard_map/ppermute | solution.py:25
  313.5 12.5 %all-to-all-start = ((bf16[4,128,256]{1,2,0:T(8,128)(2,1)}), bf16[4,128,256]{1,2,0:T(8,128)(2,1)S(1)}, u32[]{:S(2)}, u32[]{:S(2)}) async-start(bf16[4,128,256]{1,2,0:T(8,128)(2,1)} %copy.145), calls=%async_computation | async-start | bytes 524288 | tf_op jit(solution)/shard_map/all_to_all | solution.py:220
  326.0 22.3 %all-to-all-start.1 = ((bf16[4,128,256]{1,2,0:T(8,128)(2,1)}), bf16[4,128,256]{1,2,0:T(8,128)(2,1)S(1)}, u32[]{:S(2)}, u32[]{:S(2)}) async-start(bf16[4,128,256]{1,2,0:T(8,128)(2,1)} %multiply_convert_fusion.1), calls=%async_computation.1 | async-start | bytes 524288 | tf_op jit(solution)/shard_map/all_to_all | solution.py:221
  (19 other events, 149.2 us)
Sparse Core Ops, SparseCore 0:
  9.5 43.9 all-gather.12
  55.5 37.2 all-gather.16
  94.9 40.1 all-gather.20
  137.0 37.2 all-gather.22
  176.3 44.4 all-gather.28
  222.7 38.9 all-gather.26
  263.8 39.0 all-gather.14
  304.4 40.8 all-gather.18
  346.9 34.4 all-gather.24
where the time goes:
time: 395 us; the launch traced here: 392 us
  blocking collectives  103 us (26%)
  waiting for transfers between devices  101 us (26%)
  local copies, waits for them, and re-layouts  92.6 us (23%)
  matrix products  42.3 us (11%)
  other arithmetic  19.9 us (5%)
  starting transfers between devices  17.2 us (4%)
  between operations  14.6 us (4%)
    dynamic_update_slice x8, local copies, waits for them, and re-layouts, block_sweep(): lax.scan(one_block, initial, (as_blocks(readers), as_blocks(writers), as_...  35.1 us
    all_gather x1, waiting for transfers between devices, shards(): lax.all_gather(pool_cols, 'tp', axis=0, tiled=True)  33.1 us
    all_gather x1, waiting for transfers between devices, shards(): lax.all_gather(gate_matrix, 'sp', axis=0, tiled=True)  28.1 us
    all_gather x1, blocking collectives, shards(): lax.all_gather(read_matrix, 'sp', axis=0, tiled=True)  27.2 us
    all_gather x1, blocking collectives, shards(): lax.all_gather(write_matrix, 'sp', axis=0, tiled=True)  26.4 us
    all_gather x1, blocking collectives, shards(): lax.all_gather(step_matrix, 'sp', axis=0, tiled=True)  24.3 us
    unnamed x1, blocking collectives  17.8 us
    dynamic_slice x32, local copies, waits for them, and re-layouts, step(): new = combine(before, jax.tree.map(lambda part: part[at], everything))  16.8 us
  transfers between devices with their start and end apart: 15, of which 6 were waited for; matrix products, arithmetic and copies ran while one was open for 38% of the time, Pallas kernels for 0%

commit v1 on v0

v1 whole, which is shorter than its diff:
```python
import functools

import jax
import jax.numpy as jnp
from jax import lax
from jax.experimental import pallas as pl
from jax.experimental.pallas import tpu as pltpu
from jax.sharding import PartitionSpec as P

HEAD_DIM = 64
SSD_INNER = 1024
EPSILON = 1e-06
HALO = 16
LOGICAL = pl.DeviceIdType.MESH
f32 = jnp.float32
bf16 = jnp.bfloat16
HIGHEST = lax.Precision.HIGHEST


def softplus(v):
    return jnp.maximum(v, 0.0) + jnp.log1p(jnp.exp(-jnp.abs(v)))


def silu(v):
    return v / (1.0 + jnp.exp(-v))


def mixer_kernel(
    n, t_size, dims,
    tok, gain, w, stept, taps, base, psf, pld, ngain, maps, pscale,
    out,
    halo, xn, wbuf, sbuf, acc, s_out, s_in, tot_out, tot_in, ent, lea, xs, xr, qs, qr,
    w_send, w_recv, st_send, st_recv, h_send, h_recv, s_send, s_recv, t_send, t_recv,
    x_send, x_recv, q_send, q_recv,
):
    rows, inner, state, pool = dims
    me = lax.axis_index("sp")
    tp = lax.axis_index("tp")
    high = n // 2
    h, l = me // 2, me % 2
    depth = w.shape[0]
    width = tok.shape[1]

    barrier = pltpu.get_barrier_semaphore()

    def greet(k, c):
        pl.semaphore_signal(barrier, inc=1, device_id={"sp": lax.rem(me + k, n)}, device_id_type=LOGICAL)
        return c

    lax.fori_loop(1, n, greet, 0)
    for k in range(1, t_size):
        pl.semaphore_signal(barrier, inc=1, device_id={"tp": lax.rem(tp + k, t_size)}, device_id_type=LOGICAL)
    pl.semaphore_wait(barrier, n - 1 + t_size - 1)

    def w_copy(src, block, way, to):
        return pltpu.make_async_remote_copy(
            src_ref=src, dst_ref=wbuf.at[block], send_sem=w_send.at[way, block],
            recv_sem=w_recv.at[block], device_id={"sp": to}, device_id_type=LOGICAL)

    def halo_copy(side, start, to):
        return pltpu.make_async_remote_copy(
            src_ref=tok.at[pl.ds(start, HALO), :], dst_ref=halo.at[side], send_sem=h_send.at[side],
            recv_sem=h_recv.at[side], device_id={"sp": to}, device_id_type=LOGICAL)

    def st_copy(slot, to):
        return pltpu.make_async_remote_copy(
            src_ref=stept, dst_ref=sbuf.at[me], send_sem=st_send.at[to],
            recv_sem=st_recv.at[slot], device_id={"sp": to}, device_id_type=LOGICAL)

    up_ok, down_ok = h < high - 1, h > 0
    partner = me + 1 - 2 * l

    @pl.when(up_ok)
    def _():
        w_copy(w, me, 0, me + 2).start()

    @pl.when(down_ok)
    def _():
        w_copy(w, me, 1, me - 2).start()

    w_copy(w, me, 2, partner).start()

    @pl.when(me < n - 1)
    def _():
        halo_copy(0, rows - HALO, me + 1).start()

    @pl.when(me > 0)
    def _():
        halo_copy(1, 0, me - 1).start()

    def send_step(k, c):
        st_copy(me, lax.rem(me + k, n)).start()
        return c

    lax.fori_loop(1, n, send_step, 0)

    def norm(v):
        wide = v.astype(f32)
        return (wide * lax.rsqrt(jnp.mean(wide * wide, axis=1, keepdims=True) + EPSILON)
                * gain[...].astype(f32)).astype(bf16)

    chunk = 64

    def norm_rows(i, c):
        at = pl.multiple_of(i * chunk, chunk)
        xn[pl.ds(pl.multiple_of(HALO + at, HALO), chunk), :] = norm(tok[pl.ds(at, chunk), :])
        return c

    lax.fori_loop(0, rows // chunk, norm_rows, 0)

    @pl.when(me > 0)
    def _():
        halo_copy(0, 0, me).wait_recv()
        xn[0:HALO, :] = norm(halo[0])

    @pl.when(me == 0)
    def _():
        xn[0:HALO, :] = jnp.zeros((HALO, width), bf16)

    @pl.when(me < n - 1)
    def _():
        halo_copy(1, 0, me).wait_recv()
        xn[HALO + rows:, :] = norm(halo[1])

    @pl.when(me == n - 1)
    def _():
        xn[HALO + rows:, :] = jnp.zeros((HALO, width), bf16)

    def project(block, piece):
        at = pl.multiple_of(block * depth, 128)
        acc[...] += jnp.dot(xn[:, pl.ds(at, depth)], piece, preferred_element_type=f32)

    for d in range(1, high):
        @pl.when(h - d >= 0)
        def _():
            block = me - 2 * d
            w_copy(w, block, 0, me).wait_recv()

            @pl.when(up_ok)
            def _():
                w_copy(wbuf.at[block], block, 0, me + 2).start()
            w_copy(wbuf.at[block], block, 2, partner).start()

        @pl.when(h + d < high)
        def _():
            block = me + 2 * d
            w_copy(w, block, 1, me).wait_recv()

            @pl.when(down_ok)
            def _():
                w_copy(wbuf.at[block], block, 1, me - 2).start()
            w_copy(wbuf.at[block], block, 2, partner).start()

    wbuf[me] = w[...]
    sbuf[me] = stept[...]
    acc[...] = jnp.zeros_like(acc)

    def wait_cross(d, c):
        w_copy(w, 2 * d + 1 - l, 2, me).wait_recv()
        return c

    def wait_step(k, c):
        st_copy(lax.rem(me + k, n), me).wait_recv()
        return c

    lax.fori_loop(1, n, wait_step, 0)
    per = max(1, 256 // depth)

    if depth % 128 == 0:
        def own_half(i, c):
            block = 2 * lax.rem(h + i, high) + l
            project(block, wbuf[block])
            return c

        def other_half(i, c):
            d = lax.rem(h + i, high)
            wait_cross(d, 0)
            block = 2 * d + 1 - l
            project(block, wbuf[block])
            return c

        lax.fori_loop(0, high, own_half, 0)
        lax.fori_loop(0, high, other_half, 0)
    else:
        lax.fori_loop(0, high, wait_cross, 0)

        def joined(i, c):
            block = wbuf[pl.ds(i * per, per)].reshape(per * depth, wbuf.shape[2])
            at = pl.multiple_of(i * (per * depth), per * depth)
            acc[...] += jnp.dot(xn[:, pl.ds(at, per * depth)], block, preferred_element_type=f32)
            return c

        lax.fori_loop(0, n // per, joined, 0)

    stepw = jnp.concatenate([sbuf[i][:, :depth] for i in range(n)], axis=1)
    raw = lax.dot_general(stepw, xn[HALO:HALO + rows, :], (((1,), (1,)), ((), ())), preferred_element_type=f32)
    step = base[...] * softplus(raw) * psf[...]
    decay = pld[...] - step
    at_s = lax.broadcasted_iota(jnp.int32, (rows, rows), 1)
    at_t = lax.broadcasted_iota(jnp.int32, (rows, rows), 0)
    upper = (at_t <= at_s).astype(f32)
    run = lax.dot_general(decay, upper, (((1,), (0,)), ((), ())), precision=HIGHEST, preferred_element_type=f32)
    before = run - decay
    total = run[:, rows - 1:rows]
    run_c = run.T
    before_c = before.T

    acc[...] = acc[...].astype(bf16).astype(f32)
    third = inner + 2 * state
    mixed_in = (acc[HALO - 1:HALO - 1 + rows, 0:third] * taps[0:1, :].astype(f32)
                + acc[HALO:HALO + rows, 0:third] * taps[1:2, :].astype(f32)
                + acc[HALO + 1:HALO + 1 + rows, 0:third] * taps[2:3, :].astype(f32))
    active = silu(mixed_in)
    inputs = active[:, 0:inner].astype(bf16)
    writers = active[:, inner:inner + state].astype(bf16)
    readers = active[:, inner + state:third].astype(bf16)
    writers_t = writers.astype(f32).T

    heads = inner // HEAD_DIM
    lane_head = lax.broadcasted_iota(jnp.int32, (1, inner), 1) // HEAD_DIM
    picked = [jnp.where(lane_head == i, inputs.astype(f32), 0.0).astype(bf16) for i in range(heads)]

    fade = jnp.exp(total - run) * step
    lead = jnp.exp(before) * step
    s_f = jnp.zeros((state, inner), f32)
    s_b = jnp.zeros((state, inner), f32)
    tot_row = jnp.zeros((1, inner), f32)
    for i in range(heads):
        s_f += jnp.dot((writers_t * fade[i:i + 1, :]).astype(bf16), picked[i], preferred_element_type=f32)
        s_b += jnp.dot((writers_t * lead[i:i + 1, :]).astype(bf16), picked[i], preferred_element_type=f32)
        tot_row = jnp.where(lane_head == i, total[i:i + 1, :], tot_row)
    s_out[0] = s_f.astype(bf16)
    s_out[1] = s_b.astype(bf16)
    tot_out[...] = jnp.broadcast_to(tot_row, tot_out.shape)

    def s_copy(which, slot, to):
        return pltpu.make_async_remote_copy(
            src_ref=s_out.at[which], dst_ref=s_in.at[me], send_sem=s_send.at[to],
            recv_sem=s_recv.at[slot], device_id={"sp": to}, device_id_type=LOGICAL)

    def tot_copy(slot, to):
        return pltpu.make_async_remote_copy(
            src_ref=tot_out, dst_ref=tot_in.at[me], send_sem=t_send.at[to],
            recv_sem=t_recv.at[slot], device_id={"sp": to}, device_id_type=LOGICAL)

    def send_up(to, c):
        s_copy(0, me, to).start()
        tot_copy(me, to).start()
        return c

    def send_down(k, c):
        s_copy(1, me, me - 1 - k).start()
        tot_copy(me, me - 1 - k).start()
        return c

    lax.fori_loop(me + 1, n, send_up, 0)
    lax.fori_loop(0, me, send_down, 0)

    pool_at = third + inner
    half = lax.shift_left(jnp.int32(1), tp)
    ext = rows + 2 * HALO
    off = lax.broadcasted_iota(jnp.int32, (rows, ext), 1) - HALO - lax.broadcasted_iota(jnp.int32, (rows, ext), 0)
    band = jnp.where((off >= -half) & (off < half), 1.0, 0.0).astype(bf16)
    window = jnp.dot(band, acc[:, pool_at:pool_at + pool].astype(bf16), preferred_element_type=f32)
    position = me * rows + lax.broadcasted_iota(jnp.int32, (rows, 1), 0)
    count = (jnp.minimum(position + half, rows * n) - jnp.maximum(position - half, 0)).astype(f32)
    pooled = (window / count - acc[HALO:HALO + rows, pool_at:pool_at + pool]).astype(bf16)
    pool_mixed = (jnp.dot(pooled, maps[...], preferred_element_type=f32) * pscale[...].astype(f32)).astype(bf16)
    tile = rows // t_size
    for j in range(t_size):
        xs[j, :, inner:inner + pool] = pool_mixed[j * tile:(j + 1) * tile]

    scores = lax.dot_general(readers, writers, (((1,), (1,)), ((), ())), preferred_element_type=f32)
    scores = jnp.where(at_s == at_t, 2.0 * scores, scores)
    scanned = jnp.zeros((rows, inner), f32)
    for i in range(heads):
        spread = jnp.where(at_s <= at_t, run_c[:, i:i + 1] - run[i:i + 1, :],
                           before[i:i + 1, :] - before_c[:, i:i + 1])
        weights = (scores * (jnp.exp(spread) * step[i:i + 1, :])).astype(bf16)
        scanned += jnp.dot(weights, picked[i], preferred_element_type=f32)

    run_x = jnp.zeros((rows, inner), f32)
    left_x = jnp.zeros((rows, inner), f32)
    for i in range(heads):
        run_x = jnp.where(lane_head == i, run_c[:, i:i + 1], run_x)
        left_x = jnp.where(lane_head == i, total[i:i + 1, :] - before_c[:, i:i + 1], left_x)

    ent[...] = jnp.zeros_like(ent)
    lea[...] = jnp.zeros_like(lea)

    def take_wait(i):
        pltpu.make_async_remote_copy(
            src_ref=s_out.at[0], dst_ref=s_in.at[i], send_sem=s_send.at[i],
            recv_sem=s_recv.at[i], device_id={"sp": i}, device_id_type=LOGICAL).wait_recv()
        pltpu.make_async_remote_copy(
            src_ref=tot_out, dst_ref=tot_in.at[i], send_sem=t_send.at[i],
            recv_sem=t_recv.at[i], device_id={"sp": i}, device_id_type=LOGICAL).wait_recv()

    def enter(i, c):
        take_wait(i)
        ent[...] = ent[...] * jnp.exp(tot_in[i][0:1, :]) + s_in[i].astype(f32)
        return c

    def leave(k, c):
        i = n - 1 - k
        take_wait(i)
        lea[...] = lea[...] * jnp.exp(tot_in[i][0:1, :]) + s_in[i].astype(f32)
        return c

    lax.fori_loop(0, me, enter, 0)
    lax.fori_loop(0, n - 1 - me, leave, 0)
    scanned += jnp.dot(readers, ent[...].astype(bf16), preferred_element_type=f32) * jnp.exp(run_x)
    scanned += jnp.dot(readers, lea[...].astype(bf16), preferred_element_type=f32) * jnp.exp(left_x)

    gated = scanned * silu(acc[HALO:HALO + rows, third:third + inner])
    square = lax.dot_general(jnp.ones((8, inner), f32), gated * gated, (((1,), (1,)), ((), ())),
                             precision=HIGHEST, preferred_element_type=f32)
    scaled = (gated * ngain[...].astype(f32)).astype(bf16)
    for j in range(t_size):
        xs[j, :, 0:inner] = scaled[j * tile:(j + 1) * tile]
        qs[j] = square[:, j * tile:(j + 1) * tile]

    def x_copy(slot, to):
        return pltpu.make_async_remote_copy(
            src_ref=xs.at[to], dst_ref=xr.at[slot], send_sem=x_send.at[to],
            recv_sem=x_recv.at[slot], device_id={"tp": to}, device_id_type=LOGICAL)

    def q_copy(slot, to):
        return pltpu.make_async_remote_copy(
            src_ref=qs.at[to], dst_ref=qr.at[slot], send_sem=q_send.at[to],
            recv_sem=q_recv.at[slot], device_id={"tp": to}, device_id_type=LOGICAL)

    for k in range(1, t_size):
        to = lax.rem(tp + k, t_size)
        q_copy(tp, to).start()
        x_copy(tp, to).start()
    xr[tp] = xs[tp]
    qr[tp] = qs[tp]
    for k in range(1, t_size):
        frm = lax.rem(tp + k, t_size)
        q_copy(frm, frm).wait_recv()
        x_copy(frm, frm).wait_recv()
    sums = qr[0]
    for j in range(1, t_size):
        sums = sums + qr[j]
    factor = lax.rsqrt(sums.T[:, 0:1] / SSD_INNER + EPSILON)
    both = inner + pool
    for j in range(t_size):
        out[:, j * both:j * both + inner] = (xr[j, :, 0:inner].astype(f32) * factor).astype(bf16)
        out[:, j * both + inner:(j + 1) * both] = xr[j, :, inner:both]

    @pl.when(up_ok)
    def _():
        w_copy(w, me, 0, me + 2).wait_send()

    @pl.when(down_ok)
    def _():
        w_copy(w, me, 1, me - 2).wait_send()

    w_copy(w, me, 2, partner).wait_send()
    for d in range(1, high):
        @pl.when(h - d >= 0)
        def _():
            block = me - 2 * d

            @pl.when(up_ok)
            def _():
                w_copy(w, block, 0, me + 2).wait_send()
            w_copy(w, block, 2, partner).wait_send()

        @pl.when(h + d < high)
        def _():
            block = me + 2 * d

            @pl.when(down_ok)
            def _():
                w_copy(w, block, 1, me - 2).wait_send()
            w_copy(w, block, 2, partner).wait_send()

    @pl.when(me < n - 1)
    def _():
        halo_copy(0, rows - HALO, me + 1).wait_send()

    @pl.when(me > 0)
    def _():
        halo_copy(1, 0, me - 1).wait_send()

    def sent(k, c):
        to = lax.rem(me + k, n)
        st_copy(me, to).wait_send()
        s_copy(0, me, to).wait_send()
        tot_copy(me, to).wait_send()
        return c

    lax.fori_loop(1, n, sent, 0)
    for k in range(1, t_size):
        to = lax.rem(tp + k, t_size)
        q_copy(tp, to).wait_send()
        x_copy(tp, to).wait_send()


def shards(
    tokens, input_norm_gain, gate_matrix, input_matrix, write_matrix, read_matrix, step_matrix,
    pooling_input_matrix, input_conv_taps, write_conv_taps, read_conv_taps, head_step_base,
    position_step_factor, position_log_decay, gated_norm_gain, group_linear_maps,
    pooling_channel_scale, state_output_matrix, pooling_output_matrix,
):
    n, t_size = lax.axis_size("sp"), lax.axis_size("tp")
    rows, width = tokens.shape
    inner, state, pool = input_matrix.shape[1], write_matrix.shape[1], pooling_input_matrix.shape[1]
    depth = input_matrix.shape[0]
    heads = head_step_base.shape[0]
    out_w = jnp.concatenate((state_output_matrix, pooling_output_matrix), axis=0)
    out_w = lax.all_gather(out_w, "sp", axis=1, tiled=True)
    out_w = lax.all_gather(out_w, "tp", axis=0, tiled=True)

    w = jnp.concatenate((input_matrix, write_matrix, read_matrix, gate_matrix, pooling_input_matrix), axis=1)
    pad = 16 - heads
    own = lax.dynamic_slice_in_dim(step_matrix, lax.axis_index("tp") * heads, heads, 1)
    stept = jnp.pad(own.T, ((0, pad), (0, max(0, 128 - depth))))
    taps = jnp.concatenate((input_conv_taps, write_conv_taps, read_conv_taps), axis=1)
    base = jnp.pad(head_step_base, (0, pad))[:, None]
    pld = jnp.pad(position_log_decay.T, ((0, pad), (0, 0)))
    ext, cols, both = rows + 2 * HALO, w.shape[1], inner + pool
    tile = rows // t_size
    vmem = pl.BlockSpec(memory_space=pltpu.VMEM)
    dma = pltpu.SemaphoreType.DMA
    x = pl.pallas_call(
        functools.partial(mixer_kernel, n, t_size, (rows, inner, state, pool)),
        out_shape=jax.ShapeDtypeStruct((tile, t_size * both), bf16),
        in_specs=[vmem] * 11,
        out_specs=vmem,
        scratch_shapes=[
            pltpu.VMEM((2, HALO, width), bf16),
            pltpu.VMEM((ext, width), bf16),
            pltpu.VMEM((n, depth, cols), bf16),
            pltpu.VMEM((n, 16, stept.shape[1]), bf16),
            pltpu.VMEM((ext, cols), f32),
            pltpu.VMEM((2, state, inner), bf16),
            pltpu.VMEM((n, state, inner), bf16),
            pltpu.VMEM((8, inner), f32),
            pltpu.VMEM((n, 8, inner), f32),
            pltpu.VMEM((state, inner), f32),
            pltpu.VMEM((state, inner), f32),
            pltpu.VMEM((t_size, tile, both), bf16),
            pltpu.VMEM((t_size, tile, both), bf16),
            pltpu.VMEM((t_size, 8, tile), f32),
            pltpu.VMEM((t_size, 8, tile), f32),
            dma((3, n)), dma((n,)), dma((n,)), dma((n,)), dma((2,)), dma((2,)),
            dma((n,)), dma((n,)), dma((n,)), dma((n,)),
            dma((t_size,)), dma((t_size,)), dma((t_size,)), dma((t_size,)),
        ],
        compiler_params=pltpu.CompilerParams(
            collective_id=0, has_side_effects=True, vmem_limit_bytes=56 * 1024 * 1024),
        cost_estimate=pl.CostEstimate(flops=100_000_000_000, bytes_accessed=16_000_000, transcendentals=0),
    )(tokens, input_norm_gain[None, :], w, stept, taps, base, position_step_factor[None, :], pld,
      gated_norm_gain[None, :], group_linear_maps[0], pooling_channel_scale[None, :])
    return jnp.dot(x, out_w, preferred_element_type=f32).astype(bf16)


def solution(mesh):
    placed = (
        P("sp", None), P(), P("sp", "tp"), P("sp", "tp"), P("sp", "tp"), P("sp", "tp"), P("sp", None),
        P("sp", "tp"), P(None, "tp"), P(None, "tp"), P(None, "tp"), P("tp"), P("sp"), P("sp", "tp"),
        P("tp"), P("tp", None, None), P("tp"), P("tp", "sp"), P("tp", "sp"),
    )
    return jax.shard_map(
        shards, mesh=mesh, in_specs=placed, out_specs=P(("sp", "tp"), None), check_vma=False)
```

time: 395 us -> 169 us (0.43)
  blocking collectives: 103 us -> 0 us
  Pallas kernels: 0 us -> 81.7 us
  local copies, waits for them, and re-layouts: 92.6 us -> 12.4 us
  waiting for transfers between devices: 101 us -> 52.7 us
  matrix products: 42.3 us -> 5.62 us
  starting transfers between devices: 17.2 us -> 0.04 us
  other arithmetic: 19.9 us -> 3.02 us
    pallas_call x0 -> x1, Pallas kernels: none -> 81.7 us  [shards(): pl.pallas_call(functools.partial(mixer_kernel, n, t_size, (rows, inner, s...]
    all_gather x3 -> x0, blocking collectives: 77.9 us -> none  [the longest x1 27.2 us: shards(): lax.all_gather(read_matrix, 'sp', axis=0, tiled=True)]
    dynamic_update_slice x8 -> x0, local copies, waits for them, and re-layouts: 35.1 us -> none  [block_sweep(): lax.scan(one_block, initial, (as_blocks(readers), as_blocks(writers), as_...]
    all_gather x9 -> x2, waiting for transfers between devices: 87.3 us -> 52.7 us  [the longest x1 52.7 us: shards(): out_w = lax.all_gather(out_w, 'sp', axis=1, tiled=True)]
    dot_general x35 -> x1, matrix products: 37.9 us -> 5.62 us  [shards(): return jnp.dot(x, out_w, preferred_element_type=f32).astype(bf16)]
    dynamic_slice x44 -> x0, local copies, waits for them, and re-layouts: 28.4 us -> none  [the longest x32 16.8 us: step(): new = combine(before, jax.tree.map(lambda part: part[at], everything))]
    unnamed x1 -> x0, blocking collectives: 17.8 us -> none
    another operation x24 -> x0, local copies, waits for them, and re-layouts: 9.42 us -> none
  transfers between devices with their start and end apart: 15 -> 2, of which waited for: 6 -> 1; matrix products, arithmetic and copies ran while one was open for 38% -> 8% of each run, Pallas kernels for 0% -> 48%
where the time goes in v1:
time: 169 us
  Pallas kernels  81.7 us (48%)
  waiting for transfers between devices  52.7 us (31%)
  between operations  13.5 us (8%)
  local copies, waits for them, and re-layouts  12.4 us (7%)
  matrix products  5.62 us (3%)
  other arithmetic  3.02 us (2%)
    pallas_call x1, Pallas kernels, shards(): pl.pallas_call(functools.partial(mixer_kernel, n, t_size, (rows, inner, s...  81.7 us
    all_gather x1, waiting for transfers between devices, shards(): out_w = lax.all_gather(out_w, 'sp', axis=1, tiled=True)  52.7 us
    dot_general x1, matrix products, shards(): return jnp.dot(x, out_w, preferred_element_type=f32).astype(bf16)  5.62 us
    unnamed x8, local copies, waits for them, and re-layouts  4.47 us
  transfers between devices with their start and end apart: 2, of which 1 were waited for; matrix products, arithmetic and copies ran while one was open for 8% of the time, Pallas kernels for 48%

profile of v1, /device:TPU:1, one launch (start us, length us, event | category | flops | bytes accessed | tf_op | source)
XLA Modules:
  0.0 169.0 jit_solution(11351881359271287483)
XLA Ops:
  6.5 0.0 copy-start
  6.5 1.7 %pad_maximum_fusion = bf16[512,256]{1,0:T(8,128)(2,1)} fusion(bf16[256,256]{1,0:T(8,128)(2,1)} %param.37, bf16[256,256]{1,0:T(8,128)(2,1)} %param.36), kind=kLoop, calls=%fused_computation.1 | loop fusion | flops 524288 | bytes 524288 | tf_op jit(solution)/shard_map/concatenate | solution.py:413
  8.2 0.0 all-gather.3.cloned.1.call-update
  8.3 0.0 all-gather.5.cloned.1.call-start
  8.3 52.7 %all-gather.3.cloned.1.call-done = bf16[512,2048]{1,0:T(8,128)(2,1)} async-done(((bf16[512,256]{1,0:T(8,128)(2,1)}), bf16[512,2048]{1,0:T(8,128)(2,1)}) %all-gather.3.cloned.1.call-update) | async-done | bytes 2097168 | tf_op jit(solution)/shard_map/all_gather | solution.py:414
  61.0 0.0 all-gather.5.cloned.1.call-update
  61.0 1.2 broadcast_in_dim.18.ngain
  62.3 1.2 broadcast_in_dim.19.pscale
  63.5 0.7 pad_bitcast_fusion
  64.2 0.7 copy.20.base
  64.8 1.3 broadcast_in_dim.15.gain
  66.1 0.6 pad.12.stept
  66.7 1.3 pad.14.pld
  68.0 1.3 pad_maximum_fusion.1.taps
  69.4 0.9 constant_dynamic-update-slice_fusion.4
  70.3 0.9 constant_dynamic-update-slice_fusion.3
  71.2 0.9 constant_dynamic-update-slice_fusion.2
  72.1 1.0 constant_dynamic-update-slice_fusion.1
  73.0 0.9 constant_dynamic-update-slice_fusion.w
  74.0 0.0 copy-start.1
  74.0 0.8 copy-done.1
  74.8 81.7 %shard_map.181 = bf16[128,2048]{1,0:T(8,128)(2,1)} custom-call(bf16[512,2048]{1,0:T(8,128)(2,1)} %tok.1, bf16[1,2048]{1,0:T(2,128)(2,1)} %broadcast_in_dim.15.gain, bf16[256,1024]{1,0:T(8,128)(2,1)} %copy-done.1, bf16[16,256]{1,0:T(8,128)(2,1)} %pad.12.stept, bf16[3,512]{1,0:T(4,128)(2,1)} %pad_maximum_fusion.1.taps, f32[16,1]{1,0:T(8,128)} %copy.20.base, ...), custom_call_target="tpu_custom_call" | custom-call | flops 99999997952 | bytes 16000000 | tf_op jit(solution)/shard_map/pallas_call | solution.py:428
  156.5 0.0 all-gather.5.cloned.1.call-done
  156.6 5.6 %convolution_convert_fusion = bf16[128,2048]{1,0:T(8,128)(2,1)} fusion(bf16[128,2048]{1,0:T(8,128)(2,1)} %shard_map.181, bf16[2048,2048]{1,0:T(8,128)(2,1)} %all-gather.5.cloned.1.call-done), kind=kOutput, calls=%fused_computation | convolution fusion | flops 1074003968 | bytes 9437184 | tf_op jit(solution)/shard_map/dot_general | solution.py:458
  (3 shorter events, 0.0 us)
Async XLA Ops:
  6.5 59.6 %copy-start = (bf16[256,16]{0,1:T(8,128)(2,1)S(1)}, bf16[256,16]{0,1:T(8,128)(2,1)}, u32[]{:S(2)}) copy-start(bf16[256,16]{0,1:T(8,128)(2,1)} %param.25) | copy-start | bytes 24580
  6.5 54.4 %all-gather.3.cloned.1.call-start = ((), (), s32[]{:S(2)}) async-start(), calls=%async_computation | async-start | bytes 2359296 | tf_op jit(solution)/shard_map/all_gather | solution.py:414
  8.3 148.3 %all-gather.5.cloned.1.call-start = ((), (), s32[]{:S(2)}) async-start(), calls=%async_computation.1 | async-start | bytes 10485760 | tf_op jit(solution)/shard_map/all_gather | solution.py:415
  74.0 0.8 copy-start.1
Sparse Core Ops, SparseCore 0:
  9.4 51.5 all-gather.2
  62.5 57.6 all-gather.4

commit v2 on v1

--- a/solution.py
+++ b/solution.py
@@ -411,8 +411,8 @@
     depth = input_matrix.shape[0]
     heads = head_step_base.shape[0]
     out_w = jnp.concatenate((state_output_matrix, pooling_output_matrix), axis=0)
-    out_w = lax.all_gather(out_w, "sp", axis=1, tiled=True)
-    out_w = lax.all_gather(out_w, "tp", axis=0, tiled=True)
+    out_w = lax.all_gather(out_w, ("sp", "tp"), axis=0, tiled=True)
+    out_w = out_w.reshape(n, -1, out_w.shape[1])
 
     w = jnp.concatenate((input_matrix, write_matrix, read_matrix, gate_matrix, pooling_input_matrix), axis=1)
     pad = 16 - heads
@@ -455,7 +455,8 @@
         cost_estimate=pl.CostEstimate(flops=100_000_000_000, bytes_accessed=16_000_000, transcendentals=0),
     )(tokens, input_norm_gain[None, :], w, stept, taps, base, position_step_factor[None, :], pld,
       gated_norm_gain[None, :], group_linear_maps[0], pooling_channel_scale[None, :])
-    return jnp.dot(x, out_w, preferred_element_type=f32).astype(bf16)
+    mixed = jnp.einsum("tk,skc->tsc", x, out_w, preferred_element_type=f32)
+    return mixed.astype(bf16).reshape(tile, -1)
 
 
 def solution(mesh):

time: 169 us -> 146 us (0.86)
  waiting for transfers between devices: 52.7 us -> 0.04 us
  Pallas kernels: 81.7 us -> 111 us
    all_gather x2 -> x1, waiting for transfers between devices: 52.7 us -> 0.02 us  [shards(): out_w = lax.all_gather(out_w, ('sp', 'tp'), axis=0, tiled=True)]
    pallas_call x1, Pallas kernels: 81.7 us -> 111 us  [shards(): pl.pallas_call(functools.partial(mixer_kernel, n, t_size, (rows, inner, s...]
  transfers between devices with their start and end apart: 2 -> 1, of which waited for: 1 -> 0; matrix products, arithmetic and copies ran while one was open for 8% -> 9% of each run, Pallas kernels for 48% -> 76%
where the time goes in v2:
time: 146 us
  Pallas kernels  111 us (76%)
  local copies, waits for them, and re-layouts  13.6 us (9%)
  between operations  13.5 us (9%)
  matrix products  4.82 us (3%)
  other arithmetic  3.03 us (2%)
    pallas_call x1, Pallas kernels, shards(): pl.pallas_call(functools.partial(mixer_kernel, n, t_size, (rows, inner, s...  111 us
    dot_general x1, matrix products, shards(): mixed = jnp.einsum('tk,skc->tsc', x, out_w, preferred_element_type=f32)  4.82 us
    unnamed x8, local copies, waits for them, and re-layouts  4.35 us
  transfers between devices with their start and end apart: 1, of which 0 were waited for; matrix products, arithmetic and copies ran while one was open for 9% of the time, Pallas kernels for 76%

profile of v2, /device:TPU:1, one launch (start us, length us, event | category | flops | bytes accessed | tf_op | source)
XLA Modules:
  0.0 145.6 jit_solution(2553736275976226113)
XLA Ops:
  6.5 0.0 copy-start
  6.5 0.0 all-gather.2.cloned.1.call-start
  6.5 1.7 %pad_maximum_fusion = bf16[512,256]{1,0:T(8,128)(2,1)} fusion(bf16[256,256]{1,0:T(8,128)(2,1)} %param.37, bf16[256,256]{1,0:T(8,128)(2,1)} %param.36), kind=kLoop, calls=%fused_computation.2 | loop fusion | flops 524288 | bytes 524288 | tf_op jit(solution)/shard_map/concatenate | solution.py:413
  8.3 0.0 all-gather.2.cloned.1.call-update
  8.3 0.7 pad_bitcast_fusion
  9.0 0.7 copy.21.base
  9.6 1.3 broadcast_in_dim.15.gain
  10.9 1.2 broadcast_in_dim.18.ngain
  12.2 1.3 broadcast_in_dim.19.pscale
  13.4 0.6 pad.12.stept
  14.0 1.3 pad.14.pld
  15.3 1.3 pad_maximum_fusion.1.taps
  16.7 0.9 constant_dynamic-update-slice_fusion.4
  17.6 0.9 constant_dynamic-update-slice_fusion.3
  18.4 0.9 constant_dynamic-update-slice_fusion.2
  19.3 0.9 constant_dynamic-update-slice_fusion.1
  20.2 0.9 constant_dynamic-update-slice_fusion.w
  21.1 0.0 copy-start.1
  21.2 0.8 copy-done.1
  21.9 110.6 %shard_map.181 = bf16[128,2048]{1,0:T(8,128)(2,1)} custom-call(bf16[512,2048]{1,0:T(8,128)(2,1)} %tok.1, bf16[1,2048]{1,0:T(2,128)(2,1)} %broadcast_in_dim.15.gain, bf16[256,1024]{1,0:T(8,128)(2,1)} %copy-done.1, bf16[16,256]{1,0:T(8,128)(2,1)} %pad.12.stept, bf16[3,512]{1,0:T(4,128)(2,1)} %pad_maximum_fusion.1.taps, f32[16,1]{1,0:T(8,128)} %copy.21.base, ...), custom_call_target="tpu_custom_call" | custom-call | flops 99999997952 | bytes 16000000 | tf_op jit(solution)/shard_map/pallas_call | solution.py:428
  132.6 0.0 all-gather.2.cloned.1.call-done
  132.6 4.8 %convolution_convert_fusion = bf16[128,8,256]{2,0,1:T(8,128)(2,1)S(1)} fusion(bf16[8,2048,256]{2,1,0:T(8,128)(2,1)} %bitcast.13, bf16[128,2048]{1,0:T(8,128)(2,1)} %shard_map.181), kind=kOutput, calls=%fused_computation | convolution fusion | flops 1074003968 | bytes 9437184 | tf_op jit(solution)/shard_map/tk,skc->tsc/dot_general | solution.py:458
  137.4 0.3 copy.22
  137.7 1.0 copy.23
  (2 shorter events, 0.0 us)
Async XLA Ops:
  6.5 6.9 %copy-start = (bf16[256,16]{0,1:T(8,128)(2,1)S(1)}, bf16[256,16]{0,1:T(8,128)(2,1)}, u32[]{:S(2)}) copy-start(bf16[256,16]{0,1:T(8,128)(2,1)} %param.25) | copy-start | bytes 24580
  6.5 126.1 %all-gather.2.cloned.1.call-start = ((), (), s32[]{:S(2)}) async-start(), calls=%async_computation | async-start | bytes 8650752 | tf_op jit(solution)/shard_map/all_gather | solution.py:414
  21.1 0.8 copy-start.1
Sparse Core Ops, SparseCore 0:
  10.2 101.7 all-gather.1
